TPU v7x, 128 devices: a whole 4x4x4 slice. The times are simulated.
128 devices in a mesh: fs: 16 (over z, y), tp: 8 (over x, core).
Axes of the slice: x: 4, y: 4, z: 4, core: 2. Of those that a mesh axis runs over, the one named last changes fastest.
Arguments:
- tokens: bfloat16 [8192, 4096], P('fs'), may hold values from -6 to 6
- norm_gain: float32 [4096], P('fs'), may hold values from 0.1 to 1.9
- gate_train: float32 [16, 4096, 1024], P(None, 'fs', 'tp'), may hold values from -0.09375 to 0.09375
- up_train: float32 [16, 4096, 1024], P(None, 'fs', 'tp'), may hold values from -0.09375 to 0.09375
- down_train: float32 [16, 1024, 4096], P(None, 'fs', 'tp'), may hold values from -0.1875 to 0.1875
- shared_gate_train: float32 [4096, 1024], P('fs', 'tp'), may hold values from -0.09375 to 0.09375
- shared_up_train: float32 [4096, 1024], P('fs', 'tp'), may hold values from -0.09375 to 0.09375
- shared_down_train: float32 [1024, 4096], P('fs', 'tp'), may hold values from -0.1875 to 0.1875
- route_expert: int32 [8192, 2], P('fs'), may hold values from 0 to 15, all different within a row; in each aligned block of 512 rows (0 to 511, 512 to 1023, ...) at most 96 rows name the same one
- route_weight: float32 [8192, 2], P('fs'), may hold values from 0.1 to 1
Outputs:
- expert_gate: bfloat16 [16, 4096, 1024], P('fs', None, 'tp')
- expert_up: bfloat16 [16, 4096, 1024], P('fs', None, 'tp')
- expert_down: bfloat16 [16, 1024, 4096], P('fs', 'tp')
- shared_gate: bfloat16 [4096, 1024], P(None, 'tp')
- shared_up: bfloat16 [4096, 1024], P(None, 'tp')
- shared_down: bfloat16 [1024, 4096], P('tp')
- mixed: bfloat16 [8192, 4096], P('fs', 'tp')
Inputs may be any that keep to these rules, and one draw needn't show every extreme that they name: `route_expert`: each row names 2 different experts. Within each aligned block of 512 rows no expert is named by more than 96 rows, a bound that some block reaches in every draw.
All inputs are finite; a program needn't handle non-finite values.
Results may differ from a plain program's by a relative error of at most 0.015.
Values may be sent and summed in bfloat16 or wider, within the bound.
A program may use at most 128 MiB of HBM per device.

v0:
```python
import jax
import jax.numpy as jnp
from jax import lax
from jax.sharding import PartitionSpec as P

norm_eps = 1e-06


def sent_together(arrays, axis, dim, along):
    widths = [a.shape[along] for a in arrays]
    both = jnp.concatenate(arrays, axis=along)
    result = lax.all_gather(both, axis, axis=dim, tiled=True)
    return tuple(jnp.split(result, [sum(widths[:k]) for k in range(1, len(widths))], axis=along))


def blockwise_down(hidden, weight_down, pieces):
    step_width = hidden.shape[1] // pieces
    total = jnp.zeros((hidden.shape[0], weight_down.shape[1]), jnp.float32)
    for block in range(pieces):
        term = jnp.dot(
            hidden[:, block * step_width : (block + 1) * step_width],
            weight_down[block * step_width : (block + 1) * step_width],
            preferred_element_type=jnp.float32,
        )
        total = total + term.astype(jnp.bfloat16).astype(jnp.float32)
    return total


def on_device(
    tokens,
    norm_gain,
    gate_train,
    up_train,
    down_train,
    shared_gate_train,
    shared_up_train,
    shared_down_train,
    route_expert,
    route_weight,
):
    gain_rows = norm_gain[None, :, None]
    gate_local = (gain_rows * gate_train).astype(jnp.bfloat16)
    up_local = (gain_rows * up_train).astype(jnp.bfloat16)
    expert_gate, expert_up = (
        lax.all_to_all(gate_local, "fs", split_axis=0, concat_axis=1, tiled=True),
        lax.all_to_all(up_local, "fs", split_axis=0, concat_axis=1, tiled=True),
    )
    expert_down = lax.all_to_all(
        lax.all_to_all(
            down_train.astype(jnp.bfloat16), "fs", split_axis=0, concat_axis=1, tiled=True
        ),
        "tp",
        split_axis=1,
        concat_axis=2,
        tiled=True,
    )
    shared_gate_local = (norm_gain[:, None] * shared_gate_train).astype(jnp.bfloat16)
    shared_up_local = (norm_gain[:, None] * shared_up_train).astype(jnp.bfloat16)
    shared_gate, shared_up, shared_down_rows = (
        *sent_together((shared_gate_local, shared_up_local), "fs", 0, 1),
        lax.all_gather(shared_down_train.astype(jnp.bfloat16), "fs", axis=0, tiled=True),
    )
    shared_down = lax.all_to_all(shared_down_rows, "tp", split_axis=0, concat_axis=1, tiled=True)
    tok_rows, model_width = tokens.shape
    top_count = route_expert.shape[1]
    experts = lax.axis_size("fs")
    pieces = lax.axis_size("tp")
    capacity = 3 * tok_rows * top_count // (2 * experts)
    columns = model_width // pieces
    values = tokens.astype(jnp.float32)
    normed = (
        values * lax.rsqrt(jnp.mean(values * values, axis=1, keepdims=True) + norm_eps)
    ).astype(jnp.bfloat16)
    pairs = route_expert.reshape(-1)
    chosen = (pairs[:, None] == jnp.arange(experts, dtype=jnp.int32)[None, :]).astype(jnp.int32)
    earlier = jnp.cumsum(chosen, axis=0) - chosen
    slot_of = jnp.sum(earlier * chosen, axis=1)
    target = pairs * capacity + slot_of
    matches = (target[:, None] == jnp.arange(experts * capacity, dtype=jnp.int32)[None, :]).astype(
        jnp.bfloat16
    )
    placing = jnp.sum(matches.reshape(tok_rows, top_count, experts * capacity), axis=1)
    own_columns = lax.dynamic_slice_in_dim(normed, lax.axis_index("tp") * columns, columns, 1)
    outgoing = jnp.einsum("ts,td->sd", placing, own_columns, preferred_element_type=jnp.float32)
    outgoing = outgoing.astype(jnp.bfloat16).reshape(experts, capacity, columns)
    arriving = lax.all_to_all(outgoing, "fs", split_axis=0, concat_axis=0, tiled=True)
    arrived = lax.all_gather(arriving, "tp", axis=2, tiled=True)
    arrived_rows = arrived.reshape(-1, model_width)
    gate_vals = jnp.dot(arrived_rows, expert_gate[0], preferred_element_type=jnp.float32)
    up_vals = jnp.dot(arrived_rows, expert_up[0], preferred_element_type=jnp.float32)
    expert_hidden = (jax.nn.silu(gate_vals) * up_vals).astype(jnp.bfloat16)
    shared_gate_vals = jnp.dot(normed, shared_gate, preferred_element_type=jnp.float32)
    shared_up_vals = jnp.dot(normed, shared_up, preferred_element_type=jnp.float32)
    shared_hidden = (jax.nn.silu(shared_gate_vals) * shared_up_vals).astype(jnp.bfloat16)
    down_by_columns = lax.all_to_all(expert_down[0], "tp", split_axis=1, concat_axis=0, tiled=True)
    hidden_whole, shared_whole = sent_together((expert_hidden, shared_hidden), "tp", 1, 0)
    expert_sums = blockwise_down(hidden_whole, down_by_columns, pieces)
    shared_sums = blockwise_down(shared_whole, shared_down_rows, pieces)
    returning = expert_sums.astype(jnp.bfloat16).reshape(experts, capacity, columns)
    returned = lax.all_to_all(returning, "fs", split_axis=0, concat_axis=0, tiled=True).reshape(
        experts * capacity, columns
    )
    picked = jnp.take(returned, target, axis=0).reshape(tok_rows, top_count, columns)
    routed = jnp.sum(route_weight[:, :, None] * picked.astype(jnp.float32), axis=1)
    mixed = (routed + shared_sums).astype(jnp.bfloat16)
    return (expert_gate, expert_up, expert_down, shared_gate, shared_up, shared_down, mixed)


def solution(mesh):
    placed = (
        P("fs", None),
        P("fs"),
        P(None, "fs", "tp"),
        P(None, "fs", "tp"),
        P(None, "fs", "tp"),
        P("fs", "tp"),
        P("fs", "tp"),
        P("fs", "tp"),
        P("fs", None),
        P("fs", None),
    )
    return jax.shard_map(
        on_device,
        mesh=mesh,
        in_specs=placed,
        out_specs=(
            P("fs", None, "tp"),
            P("fs", None, "tp"),
            P("fs", "tp", None),
            P(None, "tp"),
            P(None, "tp"),
            P("tp", None),
            P("fs", "tp"),
        ),
        check_vma=False,
    )
```

profile of v0, /device:TPU:1, one launch (start us, length us, event | category | flops | bytes accessed | tf_op | source)
XLA Modules:
  0.0 310.7 jit_solution(5884856145658552887)
XLA Ops:
  10.2 4.5 %reduce-window.6 = s32[16,8,128]{2,1,0:T(8,128)S(1)} reduce-window(s32[16,8,128]{2,1,0:T(8,128)S(1)} %fusion.51, s32[]{:T(128)} %constant.18.clone.1), window={size=1x1x128 pad=0_0x0_0x127_0}, to_apply=%region_0.0 | reduce-window | flops 2080768 | bytes 131076 | tf_op jit(solution)/shard_map/reduce-window
  17.0 3.1 fusion
  23.6 30.3 %all_to_all.99 = bf16[16,96,512]{2,1,0:T(8,128)(2,1)} all-to-all(bf16[16,96,512]{2,1,0:T(8,128)(2,1)S(1)} %bitcast.97), channel_id=1, replica_groups=mesh['fs'=16,'tp'=8] {'fs'}, dimensions={0} | all-to-all | bytes 3145728 | tf_op jit(solution)/shard_map/all_to_all | solution.py:86
  53.9 3.5 %multiply_convert_fusion = (bf16[16,256,128]{2,1,0:T(8,128)(2,1)}, bf16[16,256,128]{2,1,0:T(8,128)(2,1)}) fusion(f32[16,256,128]{2,1,0:T(8,128)S(1)} %copy-done.11, f32[256]{0:T(256)S(1)} %copy-done.16, f32[16,256,128]{2,1,0:T(8,128)} %param.12), kind=kLoop, calls=%fused_computation.21 | loop fusion | flops 2097152 | bytes 6292480 | tf_op jit(solution)/shard_map/convert_element_type | solution.py:43
  57.5 3.9 %all-to-all-start = ((bf16[16,256,128]{2,1,0:T(8,128)(2,1)}), bf16[16,256,128]{2,1,0:T(8,128)(2,1)S(1)}, u32[]{:S(2)}, u32[]{:S(2)}) async-start(bf16[16,256,128]{2,1,0:T(8,128)(2,1)} %get-tuple-element.49), calls=%async_computation | async-start | bytes 2097152 | tf_op jit(solution)/shard_map/all_to_all | solution.py:45
  63.5 1.8 fusion.55
  68.9 6.2 %all-to-all-done = bf16[16,256,128]{2,1,0:T(8,128)(2,1)S(1)} async-done(((bf16[16,256,128]{2,1,0:T(8,128)(2,1)}), bf16[16,256,128]{2,1,0:T(8,128)(2,1)S(1)}, u32[]{:S(2)}, u32[]{:S(2)}) %all-to-all-start) | async-done | bytes 1048608 | tf_op jit(solution)/shard_map/all_to_all | solution.py:45
  75.1 3.8 %all-to-all-start.1 = ((bf16[16,256,128]{2,1,0:T(8,128)(2,1)}), bf16[16,256,128]{2,1,0:T(8,128)(2,1)S(1)}, u32[]{:S(2)}, u32[]{:S(2)}) async-start(bf16[16,256,128]{2,1,0:T(8,128)(2,1)} %get-tuple-element.48), calls=%async_computation.1 | async-start | bytes 2097152 | tf_op jit(solution)/shard_map/all_to_all | solution.py:46
  78.9 55.5 %all-gather.9.cloned.1.call-done = bf16[16,96,4096]{2,1,0:T(8,128)(2,1)} async-done(((bf16[16,96,512]{2,1,0:T(8,128)(2,1)}), bf16[16,96,4096]{2,1,0:T(8,128)(2,1)}) %all-gather.9.cloned.1.call-update) | async-done | bytes 12582928 | tf_op jit(solution)/shard_map/all_gather | solution.py:87
  134.3 6.4 %fusion.56 = f32[1536,128]{1,0:T(8,128)S(1)} fusion(bf16[1536,4096]{1,0:T(8,128)(2,1)} %bitcast.102, bf16[4096,128]{1,0:T(8,128)(2,1)S(1)} %bitcast.91), kind=kOutput, calls=%fused_computation.106 | convolution fusion | flops 1610612736 | bytes 14417920 | tf_op jit(solution)/shard_map/dot_general | solution.py:89
  140.8 7.0 %fusion.4 = bf16[1536,128]{1,0:T(8,128)(2,1)S(1)} fusion(bf16[1536,4096]{1,0:T(8,128)(2,1)} %bitcast.103, bf16[4096,128]{1,0:T(8,128)(2,1)S(1)} %bitcast.93, f32[1536,128]{1,0:T(8,128)S(1)} %fusion.56), kind=kOutput, calls=%fused_computation.19 | convolution fusion | flops 1611792384 | bytes 14811136 | tf_op jit(solution)/shard_map/dot_general | solution.py:90
  148.7 1.7 convert_element_type.153
  150.4 23.2 %all_to_all.100 = bf16[16,64,512]{2,1,0:T(8,128)(2,1)S(1)} all-to-all(bf16[16,64,512]{2,1,0:T(8,128)(2,1)S(1)} %convert_element_type.153), channel_id=1, replica_groups=mesh['fs'=16,'tp'=8] {'fs'}, dimensions={0} | all-to-all | bytes 2097152 | tf_op jit(solution)/shard_map/all_to_all | solution.py:49
  173.6 1.6 copy.87
  175.8 7.0 %reduce.1 = bf16[1024,512]{1,0:T(8,128)(2,1)S(1)} reduce(bf16[1024,1,512]{2,1,0:T(2,128)(2,1)S(1)} %bitcast.80, bf16[]{:T(256)} %broadcast.91), dimensions={1}, to_apply=%bitcast.77.reduce_sub_computation | reduce | bytes 2097154
  183.6 25.8 %all_to_all.101 = bf16[8,2,32768]{2,1,0:T(2,128)(2,1)S(1)} all-to-all(bf16[8,2,32768]{2,1,0:T(2,128)(2,1)S(1)} %reshape.154), channel_id=1, replica_groups=mesh['fs'=16,'tp'=8] {'tp'}, dimensions={0} | all-to-all | bytes 2097152 | tf_op jit(solution)/shard_map/all_to_all | solution.py:48
  209.4 5.2 %all-to-all-start.4 = ((bf16[8,128,512]{2,1,0:T(8,128)(2,1)}), bf16[8,128,512]{2,1,0:T(8,128)(2,1)}, u32[]{:S(2)}, u32[]{:S(2)}) async-start(bf16[8,128,512]{2,1,0:T(8,128)(2,1)} %bitcast.89), calls=%async_computation.4 | async-start | bytes 2097152 | tf_op jit(solution)/shard_map/all_to_all | solution.py:63
  216.9 17.0 %all-to-all-done.4 = bf16[8,128,512]{2,1,0:T(8,128)(2,1)} async-done(((bf16[8,128,512]{2,1,0:T(8,128)(2,1)}), bf16[8,128,512]{2,1,0:T(8,128)(2,1)}, u32[]{:S(2)}, u32[]{:S(2)}) %all-to-all-start.4) | async-done | bytes 1048608 | tf_op jit(solution)/shard_map/all_to_all | solution.py:63
  233.9 4.8 %all-to-all-start.6 = ((bf16[128,8,512]{2,0,1:T(8,128)(2,1)}), bf16[128,8,512]{2,0,1:T(8,128)(2,1)S(1)}, u32[]{:S(2)}, u32[]{:S(2)}) async-start(bf16[128,8,512]{2,0,1:T(8,128)(2,1)} %bitcast.14), calls=%async_computation.6 | async-start | bytes 2097152 | tf_op jit(solution)/shard_map/all_to_all | solution.py:95
  239.4 1.6 copy.71
  242.4 1.6 copy.72
  245.3 8.4 %all-to-all-done.6 = bf16[128,8,512]{2,0,1:T(8,128)(2,1)S(1)} async-done(((bf16[128,8,512]{2,0,1:T(8,128)(2,1)}), bf16[128,8,512]{2,0,1:T(8,128)(2,1)S(1)}, u32[]{:S(2)}, u32[]{:S(2)}) %all-to-all-start.6) | async-done | bytes 1048608 | tf_op jit(solution)/shard_map/all_to_all | solution.py:95
  253.7 1.7 convolution_convert_fusion.7
  255.4 1.5 convolution_convert_fusion.6
  259.7 2.8 add_convert_fusion
  262.6 3.8 %all-to-all-start.7 = ((bf16[16,96,512]{2,1,0:T(8,128)(2,1)}), bf16[16,96,512]{2,1,0:T(8,128)(2,1)S(1)}, u32[]{:S(2)}, u32[]{:S(2)}) async-start(bf16[16,96,512]{2,1,0:T(8,128)(2,1)} %bitcast.24), calls=%async_computation.7 | async-start | bytes 3145728 | tf_op jit(solution)/shard_map/all_to_all | solution.py:100
  273.5 2.2 fusion.10
  275.7 13.5 %all-to-all-done.7 = bf16[16,96,512]{2,1,0:T(8,128)(2,1)S(1)} async-done(((bf16[16,96,512]{2,1,0:T(8,128)(2,1)}), bf16[16,96,512]{2,1,0:T(8,128)(2,1)S(1)}, u32[]{:S(2)}, u32[]{:S(2)}) %all-to-all-start.7) | async-done | bytes 1572896 | tf_op jit(solution)/shard_map/all_to_all | solution.py:100
  289.2 5.1 %gather_fusion = bf16[1024,512]{1,0:T(8,128)(2,1)} fusion(bf16[1536,512]{1,0:T(8,128)(2,1)S(1)} %bitcast.78, s32[1024]{0:T(1024)S(1)} %broadcast_clamp_fusion), kind=kCustom, calls=%fused_computation | custom fusion | bytes 2101248 | tf_op jit(solution)/shard_map/jit(_take)/gather | solution.py:103
  294.3 1.6 gather.7
  295.9 4.4 %multiply_reduce_fusion = f32[512,512]{1,0:T(8,128)S(1)} fusion(bf16[512,2,512]{2,1,0:T(2,128)(2,1)S(1)} %gather.7, pred[512,2]{1,0:T(8,128)(4,1)S(1)} %copy.79, f32[512,2]{1,0:T(8,128)S(1)} %copy.73), kind=kLoop, calls=%fused_computation.20 | loop fusion | flops 1835008 | bytes 2102272 | tf_op jit(solution)/shard_map/reduce_sum | solution.py:104
  300.3 2.0 fusion.8
  (96 shorter events, 33.9 us)
Async XLA Ops:
  7.2 56.3 %all-gather.5.cloned.1.call-start = ((), (), s32[]{:S(2)}) async-start(), calls=%async_computation.8 | async-start | bytes 2228224 | tf_op jit(solution)/shard_map/all_gather | solution.py:12
  9.0 125.3 %all-gather.9.cloned.1.call-start = ((), (), s32[]{:S(2)}) async-start(), calls=%async_computation.10 | async-start | bytes 14155776 | tf_op jit(solution)/shard_map/all_gather | solution.py:87
  15.5 4.6 %copy-start = (bf16[512,4096]{1,0:T(8,128)(2,1)S(1)}, bf16[512,4096]{1,0:T(8,128)(2,1)}, u32[]{:S(2)}) copy-start(bf16[512,4096]{1,0:T(8,128)(2,1)} %param.10) | copy-start | bytes 12582916
  21.6 1.9 copy-start.1
  23.6 30.3 %copy-start.11 = (f32[16,256,128]{2,1,0:T(8,128)S(1)}, f32[16,256,128]{2,1,0:T(8,128)}, u32[]{:S(2)}) copy-start(f32[16,256,128]{2,1,0:T(8,128)} %param.13) | copy-start | bytes 6291460
  23.6 30.3 %copy-start.16 = (f32[256]{0:T(256)S(1)}, f32[256]{0:T(256)}, u32[]{:S(2)}) copy-start(f32[256]{0:T(256)} %param.11) | copy-start | bytes 3076
  53.9 7.5 %copy-start.13 = (f32[64,512]{1,0:T(8,128)S(1)}, f32[64,512]{1,0:T(8,128)}, u32[]{:S(2)}) copy-start(f32[64,512]{1,0:T(8,128)} %param.17) | copy-start | bytes 393220
  57.5 17.6 %all-to-all-start = ((bf16[16,256,128]{2,1,0:T(8,128)(2,1)}), bf16[16,256,128]{2,1,0:T(8,128)(2,1)S(1)}, u32[]{:S(2)}, u32[]{:S(2)}) async-start(bf16[16,256,128]{2,1,0:T(8,128)(2,1)} %get-tuple-element.49), calls=%async_computation | async-start | bytes 2097152 | tf_op jit(solution)/shard_map/all_to_all | solution.py:45
  61.4 148.0 %all-gather.7.cloned.1.call-start = ((), (), s32[]{:S(2)}) async-start(), calls=%async_computation.9 | async-start | bytes 1114112 | tf_op jit(solution)/shard_map/all_gather | solution.py:61
  63.5 2.9 copy-start.2
  65.3 2.3 copy-start.10
  65.3 2.3 copy-start.12
  75.1 65.7 %copy-start.5 = (bf16[16,256,128]{2,1,0:T(8,128)(2,1)}, bf16[16,256,128]{2,1,0:T(8,128)(2,1)S(1)}, u32[]{:S(2)}) copy-start(bf16[16,256,128]{2,1,0:T(8,128)(2,1)S(1)} %all-to-all-done) | copy-start | bytes 3145732
  75.1 65.7 %all-to-all-start.1 = ((bf16[16,256,128]{2,1,0:T(8,128)(2,1)}), bf16[16,256,128]{2,1,0:T(8,128)(2,1)S(1)}, u32[]{:S(2)}, u32[]{:S(2)}) async-start(bf16[16,256,128]{2,1,0:T(8,128)(2,1)} %get-tuple-element.48), calls=%async_computation.1 | async-start | bytes 2097152 | tf_op jit(solution)/shard_map/all_to_all | solution.py:46
  78.8 174.8 %all-gather.11.cloned.1.call-start = ((), (), s32[]{:S(2)}) async-start(), calls=%async_computation.11 | async-start | bytes 4718592 | tf_op jit(solution)/shard_map/all_gather | solution.py:12
  140.8 7.0 %copy-start.7 = (bf16[16,256,128]{2,1,0:T(8,128)(2,1)}, bf16[16,256,128]{2,1,0:T(8,128)(2,1)S(1)}, u32[]{:S(2)}) copy-start(bf16[16,256,128]{2,1,0:T(8,128)(2,1)S(1)} %all-to-all-done.1) | copy-start | bytes 3145732
  209.4 24.5 %all-to-all-start.4 = ((bf16[8,128,512]{2,1,0:T(8,128)(2,1)}), bf16[8,128,512]{2,1,0:T(8,128)(2,1)}, u32[]{:S(2)}, u32[]{:S(2)}) async-start(bf16[8,128,512]{2,1,0:T(8,128)(2,1)} %bitcast.89), calls=%async_computation.4 | async-start | bytes 2097152 | tf_op jit(solution)/shard_map/all_to_all | solution.py:63
  215.6 23.1 %copy-start.14 = (s32[512,2]{0,1:T(2,128)S(1)}, s32[512,2]{0,1:T(2,128)}, u32[]{:S(2)}) copy-start(s32[512,2]{0,1:T(2,128)} %param.18) | copy-start | bytes 12292
  215.6 23.6 %copy-start.15 = (f32[512,2]{0,1:T(2,128)S(1)}, f32[512,2]{0,1:T(2,128)}, u32[]{:S(2)}) copy-start(f32[512,2]{0,1:T(2,128)} %param.19) | copy-start | bytes 12292
  233.9 19.7 %all-to-all-start.6 = ((bf16[128,8,512]{2,0,1:T(8,128)(2,1)}), bf16[128,8,512]{2,0,1:T(8,128)(2,1)S(1)}, u32[]{:S(2)}, u32[]{:S(2)}) async-start(bf16[128,8,512]{2,0,1:T(8,128)(2,1)} %bitcast.14), calls=%async_computation.6 | async-start | bytes 2097152 | tf_op jit(solution)/shard_map/all_to_all | solution.py:95
  253.7 3.3 %copy-start.3 = (bf16[2048,1024]{1,0:T(8,128)(2,1)S(1)}, bf16[2048,1024]{1,0:T(8,128)(2,1)}, u32[]{:S(2)}) copy-start(bf16[2048,1024]{1,0:T(8,128)(2,1)} %all-gather.11.cloned.1.call-done) | copy-start | bytes 12582916
  262.5 3.9 %copy-start.4 = (bf16[1024,512]{1,0:T(8,128)(2,1)S(1)}, bf16[1024,512]{1,0:T(8,128)(2,1)}, u32[]{:S(2)}) copy-start(bf16[1024,512]{1,0:T(8,128)(2,1)} %all-gather.7.cloned.1.call-done) | copy-start | bytes 3145732
  262.6 26.6 %all-to-all-start.7 = ((bf16[16,96,512]{2,1,0:T(8,128)(2,1)}), bf16[16,96,512]{2,1,0:T(8,128)(2,1)S(1)}, u32[]{:S(2)}, u32[]{:S(2)}) async-start(bf16[16,96,512]{2,1,0:T(8,128)(2,1)} %bitcast.24), calls=%async_computation.7 | async-start | bytes 3145728 | tf_op jit(solution)/shard_map/all_to_all | solution.py:100
  294.3 6.0 %copy-start.9 = (f32[512,512]{1,0:T(8,128)S(1)}, f32[512,512]{1,0:T(8,128)}, u32[]{:S(2)}) copy-start(f32[512,512]{1,0:T(8,128)} %fusion.10) | copy-start | bytes 3145732
  295.8 6.4 %copy-start.6 = (bf16[16,256,128]{2,1,0:T(8,128)(2,1)S(1)}, bf16[16,256,128]{2,1,0:T(8,128)(2,1)}, u32[]{:S(2)}) copy-start(bf16[16,256,128]{2,1,0:T(8,128)(2,1)} %copy-done.5) | copy-start | bytes 3145732
  295.8 7.4 %copy-start.8 = (bf16[16,256,128]{2,1,0:T(8,128)(2,1)S(1)}, bf16[16,256,128]{2,1,0:T(8,128)(2,1)}, u32[]{:S(2)}) copy-start(bf16[16,256,128]{2,1,0:T(8,128)(2,1)} %copy-done.7) | copy-start | bytes 3145732
Sparse Core Ops, SparseCore 0:
  10.7 52.7 all-gather.4
  65.1 69.1 all-gather.8
  137.1 43.5 all-gather.6
  182.8 53.8 all-gather.10
where the time goes:
time: 313 us; the launch traced here: 311 us
  waiting for transfers between devices  102 us (33%)
  blocking collectives  79.3 us (25%)
  matrix products  37 us (12%)
  other arithmetic  30.7 us (10%)
  local copies, waits for them, and re-layouts  25.9 us (8%)
  starting transfers between devices  21.6 us (7%)
  between operations  14.3 us (5%)
    all_gather x1, waiting for transfers between devices, on_device(): arrived = lax.all_gather(arriving, 'tp', axis=2, tiled=True)  55.5 us
    all_to_all x1, blocking collectives, on_device(): lax.all_to_all(outgoing, 'fs', split_axis=0, concat_axis=0, tiled=True)  30.3 us
    all_to_all x1, blocking collectives, on_device(): lax.all_to_all(lax.all_to_all(down_train.astype(jnp.bfloat16), 'fs', spli...  25.8 us
    all_to_all x1, blocking collectives, on_device(): lax.all_to_all(down_train.astype(jnp.bfloat16), 'fs', split_axis=0, conca...  23.2 us
    dot_general x16, matrix products, blockwise_down(): jnp.dot(hidden[:, block * step_width:(block + 1) * step_width], weight_do...  20.1 us
    all_to_all x1, waiting for transfers between devices, on_device(): lax.all_to_all(shared_down_rows, 'tp', split_axis=0, concat_axis=1, tiled...  17 us
    all_to_all x1, waiting for transfers between devices, on_device(): lax.all_to_all(returning, 'fs', split_axis=0, concat_axis=0, tiled=True)  13.5 us
    unnamed x44, local copies, waits for them, and re-layouts  11.2 us
  transfers between devices with their start and end apart: 9, of which 6 were waited for; matrix products, arithmetic and copies ran while one was open for 21% of the time, Pallas kernels for 0%

commit v1 on v0

v1 whole, which is shorter than its diff:
```python
import jax
import jax.numpy as jnp
from jax import lax
from jax.experimental import pallas as pl
from jax.experimental.pallas import tpu as pltpu
from jax.sharding import PartitionSpec as P

norm_eps = 1e-06
MESH = pl.DeviceIdType.MESH
F32 = jnp.float32
BF16 = jnp.bfloat16
CAP = 96
GROUP = 4 * CAP
HALF = GROUP // 2
TOK = 512
D = 4096
COL = 512
H = 1024
HB = 128
ROWS = 16 * CAP
ORDER = (0, 1, 3, 2)
NEAR = [(a, b) for a in ORDER for b in ORDER if (a, b) != (0, 0)]
FAR = NEAR[::-1]


def dot(a, b):
    return jnp.dot(a, b, preferred_element_type=F32)


def kernel(
    tok_in,
    gain_in,
    gate_in,
    up_in,
    dn_in,
    shg_in,
    shu_in,
    shd_in,
    route,
    weight,
    eg_out,
    eu_out,
    ed_out,
    sg_out,
    su_out,
    sd_out,
    mix_out,
    tok,
    gate_f,
    up_f,
    dn_f,
    shg_f,
    shu_f,
    shd_f,
    gain_col,
    scale_col,
    own,
    outgoing,
    arrived,
    gu_send,
    gu,
    dn_send,
    dcol,
    drow,
    shgu,
    sdcol,
    sdrow,
    acc,
    hid,
    rsend,
    ret,
    comb,
    macc,
    mixv,
    ss,
    rs,
    ls,
    os,
):
    f = lax.axis_index("fs")
    c = lax.axis_index("tp")
    z, y = f // 4, f % 4
    x, k = c // 2, c % 2

    def fs_of(oz, oy):
        return ((z + oz) % 4) * 4 + (y + oy) % 4

    def tp_of(d, other=0):
        return ((x + d) % 4) * 2 + (k + other) % 2

    def fs_dev(oz, oy):
        return (fs_of(oz, oy), c)

    def tp_dev(d, other=0):
        return (f, tp_of(d, other))

    partner = tp_dev(0, 1)
    sent = []
    keys = {}

    def place(key):
        return keys.setdefault(key, len(keys))

    def send(src, dst, key, dev):
        copy = pltpu.make_async_remote_copy(
            src_ref=src,
            dst_ref=dst,
            send_sem=ss.at[len(sent)],
            recv_sem=rs.at[place(key)],
            device_id=dev,
            device_id_type=MESH,
        )
        copy.start()
        sent.append(copy)

    def arrive(dst, key):
        pltpu.make_async_remote_copy(
            src_ref=dst,
            dst_ref=dst,
            send_sem=ss.at[0],
            recv_sem=rs.at[place(key)],
            device_id=partner,
            device_id_type=MESH,
        ).wait_recv()

    def cols(tp_index, width):
        return pl.ds(pl.multiple_of(tp_index * width, width), width)

    def block(index, width):
        return pl.ds(pl.multiple_of(index * width, width), width)

    loads = {}
    for n, (name, src, dst) in enumerate(
        (
            ("tok", tok_in, tok),
            ("gate", gate_in, gate_f),
            ("up", up_in, up_f),
            ("shg", shg_in, shg_f),
            ("shu", shu_in, shu_f),
            ("dn", dn_in, dn_f),
            ("shd", shd_in, shd_f),
        )
    ):
        loads[name] = pltpu.make_async_copy(src, dst, ls.at[n])
        loads[name].start()

    barrier = pltpu.get_barrier_semaphore()
    for oz, oy in NEAR:
        pl.semaphore_signal(barrier, inc=1, device_id=fs_dev(oz, oy), device_id_type=MESH)
    for d in range(4):
        for other in range(2):
            if (d, other) != (0, 0):
                pl.semaphore_signal(
                    barrier, inc=1, device_id=tp_dev(d, other), device_id_type=MESH
                )

    r0, r1 = route[0:1, :], route[1:2, :]
    e_row = lax.broadcasted_iota(jnp.int32, (16, TOK), 0)
    is0, is1 = e_row == r0, e_row == r1
    named = jnp.where(is0 | is1, 1.0, 0.0).astype(BF16)
    before = jnp.where(
        lax.broadcasted_iota(jnp.int32, (TOK, TOK), 0)
        < lax.broadcasted_iota(jnp.int32, (TOK, TOK), 1),
        1.0,
        0.0,
    ).astype(BF16)
    earlier = dot(named, before)

    def target_of(r, hit):
        slot = jnp.sum(jnp.where(hit, earlier, 0.0), axis=0, keepdims=True)
        relative = (((r // 4) - z + 4) % 4) * 4 + ((r % 4) - y + 4) % 4
        return relative.astype(F32) * float(CAP) + slot

    t0, t1 = target_of(r0, is0), target_of(r1, is1)

    diag = lax.broadcasted_iota(jnp.int32, (256, 256), 0) == lax.broadcasted_iota(
        jnp.int32, (256, 256), 1
    )
    gain_col[...] = jnp.broadcast_to(
        jnp.sum(jnp.where(diag, gain_in[...], 0.0), axis=1, keepdims=True), (256, HB)
    )

    loads["tok"].wait()

    def scale_step(i, carry):
        rows = pl.ds(pl.multiple_of(i * 16, 16), 16)
        v = tok[rows, :].astype(F32)
        s = lax.rsqrt(jnp.sum(v * v, axis=1, keepdims=True) * (1.0 / D) + norm_eps)
        scale_col[rows, :] = jnp.broadcast_to(s, (16, HB))
        mine = tok[rows, cols(c, COL)].astype(F32)
        own[rows, :] = (mine * s).astype(BF16)
        return carry

    lax.fori_loop(0, TOK // 16, scale_step, 0)

    for n, g in enumerate(ORDER):
        s_row = (lax.broadcasted_iota(jnp.int32, (GROUP, TOK), 0) + g * GROUP).astype(F32)
        placing = jnp.where((s_row == t0) | (s_row == t1), 1.0, 0.0).astype(BF16)
        outgoing[g * GROUP : (g + 1) * GROUP, :] = dot(placing, own[...]).astype(BF16)
        if n == 0:
            pl.semaphore_wait(barrier, 22)
        for dy in ORDER:
            if (g, dy) != (0, 0):
                there = ((4 - g) % 4) * 4 + (4 - dy) % 4
                send(
                    outgoing.at[pl.ds((g * 4 + dy) * CAP, CAP)],
                    arrived.at[pl.ds(there * CAP, CAP), cols(c, COL)],
                    ("tok", there),
                    fs_dev(g, dy),
                )
    arrived[0:CAP, cols(c, COL)] = outgoing[0:CAP, :]

    loads["gate"].wait()
    loads["up"].wait()

    def gu_step(e, carry):
        gu_send[e, :, 0:HB] = (gate_f[e] * gain_col[...]).astype(BF16)
        gu_send[e, :, HB : 2 * HB] = (up_f[e] * gain_col[...]).astype(BF16)
        return carry

    lax.fori_loop(0, 16, gu_step, 0)
    for part in range(2):
        for oz, oy in FAR:
            there = ((4 - oz) % 4) * 4 + (4 - oy) % 4
            send(
                gu_send.at[fs_of(oz, oy), pl.ds(part * 128, 128)],
                gu.at[pl.ds(pl.multiple_of(f * 256 + part * 128, 128), 128)],
                ("gu", part, there),
                fs_dev(oz, oy),
            )
    gu[block(f, 256), :] = gu_send[f]

    def token_first(g):
        for dy in ORDER:
            if (g, dy) != (0, 0):
                s = g * 4 + dy
                arrive(arrived.at[pl.ds(s * CAP, CAP), cols(c, COL)], ("tok", s))
        piece = arrived.at[pl.ds(g * GROUP, GROUP), cols(c, COL)]
        send(piece, piece, ("xm", g), tp_dev(1))
        send(piece, piece, ("xp", g), tp_dev(3))
        send(piece, piece, ("kp", g, 0), partner)

    def token_second(g):
        for name, d, then, on, start in (("xm", 3, "ft", 1, 0), ("xp", 1, "fb", 3, HALF)):
            piece = arrived.at[pl.ds(g * GROUP, GROUP), cols(tp_of(d), COL)]
            arrive(piece, (name, g))
            part = arrived.at[pl.ds(g * GROUP + start, HALF), cols(tp_of(d), COL)]
            send(part, part, (then, g), tp_dev(on))
            send(piece, piece, ("kp", g, d), partner)

    def token_third(g):
        for name, start in (("ft", 0), ("fb", HALF)):
            part = arrived.at[pl.ds(g * GROUP + start, HALF), cols(tp_of(2), COL)]
            arrive(part, (name, g))
        piece = arrived.at[pl.ds(g * GROUP, GROUP), cols(tp_of(2), COL)]
        send(piece, piece, ("kp", g, 2), partner)

    def silu_times(gate, up):
        return (gate / (1.0 + jnp.exp(-gate)) * up).astype(BF16)

    def hidden_out(g, rows):
        piece = hid.at[rows, cols(c, HB)]
        for d in (1, 3, 2):
            send(piece, piece, ("hx", g, 4 - d), tp_dev(d))
        send(piece, piece, ("hk", g, 0), partner)

    def hidden_rows(g):
        return pl.ds(g * GROUP, GROUP) if g < 4 else pl.ds(ROWS, TOK)

    def expert_hidden(g):
        for d in range(4):
            piece = arrived.at[pl.ds(g * GROUP, GROUP), cols(tp_of(d, 1), COL)]
            arrive(piece, ("kp", g, d))
        rows = pl.ds(g * GROUP, GROUP)
        acc[0:GROUP] = jnp.zeros((GROUP, 2 * HB), F32)

        def step(i, carry):
            acc[0:GROUP] += dot(arrived[rows, block(i, COL)], gu[block(i, COL), :])
            return carry

        lax.fori_loop(0, 8, step, 0)
        hid[rows, cols(c, HB)] = silu_times(acc[0:GROUP, 0:HB], acc[0:GROUP, HB:])
        hidden_out(g, rows)

    def hidden_second(g):
        rows = hidden_rows(g)
        for d in (1, 3, 2):
            piece = hid.at[rows, cols(tp_of(d), HB)]
            arrive(piece, ("hx", g, d))
            send(piece, piece, ("hk", g, d), partner)

    def hidden_last(g):
        rows = hidden_rows(g)
        for d in range(4):
            arrive(hid.at[rows, cols(tp_of(d, 1), HB)], ("hk", g, d))

    def expert_down(g):
        hidden_last(g)
        rows = pl.ds(g * GROUP, GROUP)
        rsend[rows, :] = dot(hid[rows, :], dcol[...]).astype(BF16)
        for dy in ORDER:
            if (g, dy) != (0, 0):
                there = ((4 - g) % 4) * 4 + (4 - dy) % 4
                send(
                    rsend.at[pl.ds((g * 4 + dy) * CAP, CAP)],
                    ret.at[pl.ds(there * CAP, CAP)],
                    ("ret", there),
                    fs_dev(g, dy),
                )
        if g == 0:
            ret[0:CAP, :] = rsend[0:CAP, :]

    def line(j, d):
        return fs_of(k * j + (1 - k) * d, (1 - k) * j + k * d)

    def spread_first(name, ref, height):
        piece = ref.at[block(f, height)]
        for d in (1, 3, 2):
            send(piece, piece, (name, 4 - d), (line(d, 0), c))

    def spread_second(name, ref, height):
        for j in (0, 1, 3, 2):
            piece = ref.at[block(line(j, 0), height)]
            if j:
                arrive(piece, (name, j))
            for d in (1, 3, 2):
                send(piece, piece, (name, j, 4 - d), (line(0, d), c))

    def spread_last(name, ref, height):
        for j in range(4):
            for d in (1, 2, 3):
                arrive(ref.at[block(line(j, d), height)], (name, j, d))

    def across(name, src, dst):
        for d in (1, 3, 2, 0):
            for other in range(2):
                if (d, other) != (0, 0):
                    send(
                        src.at[cols(tp_of(d, other), HB)],
                        dst.at[:, cols(c, COL)],
                        (name, (4 - d) % 4, other),
                        tp_dev(d, other),
                    )
        dst[:, cols(c, COL)] = src[cols(c, HB), :]

    def across_last(name, dst):
        for d in range(4):
            for other in range(2):
                if (d, other) != (0, 0):
                    arrive(dst.at[:, cols(tp_of(d, other), COL)], (name, d, other))

    writes = []

    def write(src, dst):
        copy = pltpu.make_async_copy(src, dst, os.at[len(writes)])
        copy.start()
        writes.append(copy)

    loads["shg"].wait()
    loads["shu"].wait()
    shgu[block(f, 256), 0:HB] = (shg_f[...] * gain_col[...]).astype(BF16)
    shgu[block(f, 256), HB : 2 * HB] = (shu_f[...] * gain_col[...]).astype(BF16)
    token_first(0)
    spread_first("sh", shgu, 256)

    loads["dn"].wait()

    def dn_step(e, carry):
        dn_send[e] = dn_f[e].astype(BF16)
        return carry

    lax.fori_loop(0, 16, dn_step, 0)
    for oz, oy in FAR:
        there = ((4 - oz) % 4) * 4 + (4 - oy) % 4
        send(dn_send.at[fs_of(oz, oy)], dcol.at[block(f, 64)], ("dn", there), fs_dev(oz, oy))
    dcol[block(f, 64), :] = dn_send[f]
    loads["shd"].wait()
    sdcol[block(f, 64), :] = shd_f[...].astype(BF16)
    spread_first("sd", sdcol, 64)

    def norm_step(i, carry):
        rows = pl.ds(pl.multiple_of(i * 16, 16), 16)
        tok[rows, :] = (tok[rows, :].astype(F32) * scale_col[rows, 0:1]).astype(BF16)
        return carry

    lax.fori_loop(0, TOK // 16, norm_step, 0)

    token_first(1)
    token_second(0)
    token_first(3)
    token_second(1)
    token_third(0)
    token_first(2)

    packed = jnp.concatenate([t0, t1, weight[...], jnp.zeros((4, TOK), F32)], axis=0)
    by_token = packed.T
    for g in range(4):
        s_col = (lax.broadcasted_iota(jnp.int32, (TOK, GROUP), 1) + g * GROUP).astype(F32)
        comb[:, g * GROUP : (g + 1) * GROUP] = (
            jnp.where(s_col == by_token[:, 0:1], by_token[:, 2:3], 0.0)
            + jnp.where(s_col == by_token[:, 1:2], by_token[:, 3:4], 0.0)
        ).astype(BF16)

    token_second(3)
    token_third(1)
    spread_second("sh", shgu, 256)
    spread_second("sd", sdcol, 64)
    for part in range(2):
        for oz, oy in NEAR:
            arrive(
                gu.at[pl.ds(pl.multiple_of(fs_of(oz, oy) * 256 + part * 128, 128), 128)],
                ("gu", part, oz * 4 + oy),
            )
    write(gu.at[:, pl.ds(0, HB)], eg_out.at[0])
    write(gu.at[:, pl.ds(HB, HB)], eu_out.at[0])
    expert_hidden(0)
    token_second(2)
    token_third(3)
    expert_hidden(1)
    hidden_second(0)
    token_third(2)
    expert_hidden(3)
    hidden_second(1)

    spread_last("sh", shgu, 256)
    write(shgu.at[:, pl.ds(0, HB)], sg_out)
    write(shgu.at[:, pl.ds(HB, HB)], su_out)
    acc[...] = jnp.zeros((TOK, 2 * HB), F32)

    def shared_step(i, carry):
        acc[...] += dot(tok[:, block(i, COL)], shgu[block(i, COL), :])
        return carry

    lax.fori_loop(0, 8, shared_step, 0)
    hid[ROWS : ROWS + TOK, cols(c, HB)] = silu_times(acc[:, 0:HB], acc[:, HB:])
    expert_hidden(2)
    hidden_out(4, hidden_rows(4))
    hidden_second(3)
    for oz, oy in NEAR:
        arrive(dcol.at[block(fs_of(oz, oy), 64)], ("dn", oz * 4 + oy))
    expert_down(0)
    across("dx", dcol, drow)
    expert_down(1)
    hidden_second(2)
    expert_down(3)
    hidden_second(4)
    expert_down(2)

    spread_last("sd", sdcol, 64)
    across("sx", sdcol, sdrow)
    hidden_last(4)
    macc[...] = dot(hid[ROWS : ROWS + TOK, :], sdcol[...])
    for g in ORDER:
        oz = (4 - g) % 4
        for oy in ORDER:
            if (oz, oy) != (0, 0):
                s = oz * 4 + oy
                arrive(ret.at[pl.ds(s * CAP, CAP)], ("ret", s))
        macc[...] += dot(comb[:, oz * GROUP : (oz + 1) * GROUP], ret[oz * GROUP : (oz + 1) * GROUP])
    mixv[...] = macc[...].astype(BF16)
    write(mixv, mix_out)
    across_last("dx", drow)
    write(drow, ed_out.at[0])
    across_last("sx", sdrow)
    write(sdrow, sd_out)
    for copy in sent:
        copy.wait_send()
    for copy in writes:
        copy.wait()


def on_device(
    tokens,
    norm_gain,
    gate_train,
    up_train,
    down_train,
    shared_gate_train,
    shared_up_train,
    shared_down_train,
    route_expert,
    route_weight,
):
    hbm = pl.BlockSpec(memory_space=pl.ANY)
    vmem = pl.BlockSpec(memory_space=pltpu.VMEM)
    return pl.pallas_call(
        kernel,
        out_shape=(
            jax.ShapeDtypeStruct((1, D, HB), BF16),
            jax.ShapeDtypeStruct((1, D, HB), BF16),
            jax.ShapeDtypeStruct((1, HB, D), BF16),
            jax.ShapeDtypeStruct((D, HB), BF16),
            jax.ShapeDtypeStruct((D, HB), BF16),
            jax.ShapeDtypeStruct((HB, D), BF16),
            jax.ShapeDtypeStruct((TOK, COL), BF16),
        ),
        in_specs=[hbm, vmem, hbm, hbm, hbm, hbm, hbm, hbm, vmem, vmem],
        out_specs=(hbm,) * 7,
        scratch_shapes=[
            pltpu.VMEM((TOK, D), BF16),
            pltpu.VMEM((16, 256, HB), F32),
            pltpu.VMEM((16, 256, HB), F32),
            pltpu.VMEM((16, 64, COL), F32),
            pltpu.VMEM((256, HB), F32),
            pltpu.VMEM((256, HB), F32),
            pltpu.VMEM((64, COL), F32),
            pltpu.VMEM((256, HB), F32),
            pltpu.VMEM((TOK, HB), F32),
            pltpu.VMEM((TOK, COL), BF16),
            pltpu.VMEM((ROWS, COL), BF16),
            pltpu.VMEM((ROWS, D), BF16),
            pltpu.VMEM((16, 256, 2 * HB), BF16),
            pltpu.VMEM((D, 2 * HB), BF16),
            pltpu.VMEM((16, 64, COL), BF16),
            pltpu.VMEM((H, COL), BF16),
            pltpu.VMEM((HB, D), BF16),
            pltpu.VMEM((D, 2 * HB), BF16),
            pltpu.VMEM((H, COL), BF16),
            pltpu.VMEM((HB, D), BF16),
            pltpu.VMEM((TOK, 2 * HB), F32),
            pltpu.VMEM((ROWS + TOK, H), BF16),
            pltpu.VMEM((ROWS, COL), BF16),
            pltpu.VMEM((ROWS, COL), BF16),
            pltpu.VMEM((TOK, ROWS), BF16),
            pltpu.VMEM((TOK, COL), F32),
            pltpu.VMEM((TOK, COL), BF16),
            pltpu.SemaphoreType.DMA((192,)),
            pltpu.SemaphoreType.DMA((192,)),
            pltpu.SemaphoreType.DMA((7,)),
            pltpu.SemaphoreType.DMA((7,)),
        ],
        compiler_params=pltpu.CompilerParams(
            collective_id=0, has_side_effects=True, vmem_limit_bytes=62 * 1024 * 1024
        ),
        name="layer",
    )(
        tokens,
        norm_gain.reshape(1, 256),
        gate_train,
        up_train,
        down_train,
        shared_gate_train,
        shared_up_train,
        shared_down_train,
        route_expert.T,
        route_weight.T,
    )


def solution(mesh):
    placed = (
        P("fs", None),
        P("fs"),
        P(None, "fs", "tp"),
        P(None, "fs", "tp"),
        P(None, "fs", "tp"),
        P("fs", "tp"),
        P("fs", "tp"),
        P("fs", "tp"),
        P("fs", None),
        P("fs", None),
    )
    return jax.shard_map(
        on_device,
        mesh=mesh,
        in_specs=placed,
        out_specs=(
            P("fs", None, "tp"),
            P("fs", None, "tp"),
            P("fs", "tp", None),
            P(None, "tp"),
            P(None, "tp"),
            P("tp", None),
            P("fs", "tp"),
        ),
        check_vma=False,
    )
```

time: 313 us -> 145 us (0.46)
  Pallas kernels: 0 us -> 135 us
  waiting for transfers between devices: 102 us -> 0 us
  blocking collectives: 79.3 us -> 0 us
  matrix products: 37 us -> 0 us
  other arithmetic: 30.7 us -> 0 us
  starting transfers between devices: 21.6 us -> 0 us
  local copies, waits for them, and re-layouts: 25.9 us -> 8.07 us
  between operations: 14.3 us -> 0.67 us
    pallas_call x0 -> x1, Pallas kernels: none -> 135 us  [on_device(): pl.pallas_call(kernel, out_shape=(jax.ShapeDtypeStruct((1, D, HB), BF16),...]
    all_to_all x3 -> x0, blocking collectives: 79.3 us -> none  [the longest x1 30.3 us: on_device(): lax.all_to_all(outgoing, 'fs', split_axis=0, concat_axis=0, tiled=True)]
    all_gather x4 -> x0, waiting for transfers between devices: 56.8 us -> none  [the longest x1 55.5 us: on_device(): arrived = lax.all_gather(arriving, 'tp', axis=2, tiled=True)]
    all_to_all x5 -> x0, waiting for transfers between devices: 45 us -> none  [the longest x1 17 us: on_device(): lax.all_to_all(shared_down_rows, 'tp', split_axis=0, concat_axis=1, tiled...]
    dot_general x21 -> x0, matrix products: 37 us -> none  [the longest x16 20.1 us: blockwise_down(): jnp.dot(hidden[:, block * step_width:(block + 1) * step_width], weight_do...]
    all_to_all x5 -> x0, starting transfers between devices: 21.5 us -> none  [the longest x1 5.16 us: on_device(): lax.all_to_all(shared_down_rows, 'tp', split_axis=0, concat_axis=1, tiled...]
    convert_element_type x6 -> x0, other arithmetic: 8.5 us -> none  [the longest x1 3.54 us: on_device(): up_local = (gain_rows * up_train).astype(jnp.bfloat16)]
    reduce_sum x4 -> x0, other arithmetic: 8.11 us -> none  [the longest x1 4.38 us: on_device(): jnp.sum(route_weight[:, :, None] * picked.astype(jnp.float32), axis=1)]
  transfers between devices with their start and end apart: 9 -> 0, of which waited for: 6 -> 0; matrix products, arithmetic and copies ran while one was open for 21% -> 0% of each run, Pallas kernels for 0% -> 0%
where the time goes in v1:
time: 145 us; the launch traced here: 144 us
  Pallas kernels  135 us (93%)
  local copies, waits for them, and re-layouts  8.07 us (6%)
    pallas_call x1, Pallas kernels, on_device(): pl.pallas_call(kernel, out_shape=(jax.ShapeDtypeStruct((1, D, HB), BF16),...  135 us
    unnamed x19, local copies, waits for them, and re-layouts  8.07 us

profile of v1, /device:TPU:1, one launch (start us, length us, event | category | flops | bytes accessed | tf_op | source)
XLA Modules:
  0.0 143.8 jit_solution(11457710714319677969)
XLA Ops:
  0.6 135.1 %layer.1 = (bf16[1,4096,128]{2,1,0:T(8,128)(2,1)}, bf16[1,4096,128]{2,1,0:T(8,128)(2,1)}, bf16[1,128,4096]{2,1,0:T(8,128)(2,1)}, bf16[4096,128]{1,0:T(8,128)(2,1...) custom-call(bf16[512,4096]{1,0:T(8,128)(2,1)} %tok_in.1, f32[1,256]{1,0:T(1,128)} %bitcast.5, ...), custom_call_target="tpu_custom_call" | custom-call | tf_op jit(solution)/shard_map/layer/pallas_call | solution.py:486
  135.7 0.0 copy-start.4
  135.7 0.0 copy-start.3
  135.7 2.4 %copy.24 = bf16[1,4096,128]{2,1,0:T(8,128)(2,1)} copy(bf16[1,4096,128]{2,1,0:T(8,128)(2,1)} %get-tuple-element.14) | data formatting | bytes 2097152
  138.2 0.0 copy-done.4
  138.2 0.0 copy-start.2
  138.2 1.0 copy.25
  139.1 0.0 copy-done.3
  139.1 0.0 copy-start.1
  139.1 1.0 copy.26
  140.1 0.0 copy-done.2
  140.1 0.0 copy-start
  140.1 1.0 copy.27
  141.1 0.0 copy-done.1
  141.1 0.0 copy-start.5
  141.1 1.0 copy.28
  142.1 0.0 copy-done
  142.1 1.0 copy.29
  143.0 0.0 copy-done.5
  143.0 0.8 copy.30
Async XLA Ops:
  135.7 2.4 %copy-start.4 = (bf16[1,4096,128]{2,1,0:T(8,128)(2,1)S(1)}, bf16[1,4096,128]{2,1,0:T(8,128)(2,1)}, u32[]{:S(2)}) copy-start(bf16[1,4096,128]{2,1,0:T(8,128)(2,1)} %get-tuple-element.15) | copy-start | bytes 3145732
  135.7 3.4 %copy-start.3 = (bf16[1,128,4096]{2,1,0:T(8,128)(2,1)S(1)}, bf16[1,128,4096]{2,1,0:T(8,128)(2,1)}, u32[]{:S(2)}) copy-start(bf16[1,128,4096]{2,1,0:T(8,128)(2,1)} %get-tuple-element.16) | copy-start | bytes 3145732
  138.2 1.9 %copy-start.2 = (bf16[4096,128]{1,0:T(8,128)(2,1)S(1)}, bf16[4096,128]{1,0:T(8,128)(2,1)}, u32[]{:S(2)}) copy-start(bf16[4096,128]{1,0:T(8,128)(2,1)} %get-tuple-element.17) | copy-start | bytes 3145732
  139.1 1.9 %copy-start.1 = (bf16[4096,128]{1,0:T(8,128)(2,1)S(1)}, bf16[4096,128]{1,0:T(8,128)(2,1)}, u32[]{:S(2)}) copy-start(bf16[4096,128]{1,0:T(8,128)(2,1)} %get-tuple-element.18) | copy-start | bytes 3145732
  140.1 1.9 %copy-start = (bf16[128,4096]{1,0:T(8,128)(2,1)S(1)}, bf16[128,4096]{1,0:T(8,128)(2,1)}, u32[]{:S(2)}) copy-start(bf16[128,4096]{1,0:T(8,128)(2,1)} %get-tuple-element.19) | copy-start | bytes 3145732
  141.1 1.9 %copy-start.5 = (bf16[512,512]{1,0:T(8,128)(2,1)S(1)}, bf16[512,512]{1,0:T(8,128)(2,1)}, u32[]{:S(2)}) copy-start(bf16[512,512]{1,0:T(8,128)(2,1)} %get-tuple-element.20) | copy-start | bytes 1572868

commit v2 on v1

v2 whole, which is shorter than its diff:
```python
import jax
import jax.numpy as jnp
from jax import lax
from jax.experimental import pallas as pl
from jax.experimental.pallas import tpu as pltpu
from jax.sharding import PartitionSpec as P

norm_eps = 1e-06
MESH = pl.DeviceIdType.MESH
F32 = jnp.float32
BF16 = jnp.bfloat16
CAP = 96
GROUP = 4 * CAP
HALF = GROUP // 2
TOK = 512
D = 4096
COL = 512
H = 1024
HB = 128
ROWS = 16 * CAP
ORDER = (0, 1, 3, 2)
NEAR = [(a, b) for a in ORDER for b in ORDER if (a, b) != (0, 0)]
FAR = NEAR[::-1]
CHUNKS = ((0, CAP), (CAP, 3 * CAP), (GROUP, GROUP), (3 * GROUP, GROUP), (2 * GROUP, GROUP))

PLAN = (
    "t1:1", "t2:0", "t1:2", "t2:1", "t3:0", "sd2", "t1:3", "t2:2", "t3:1", "comb", "norm",
    "t1:4", "t2:3", "t3:2", "t2:4", "t3:3", "gu", "eh:0", "eh:1", "t3:4", "eh:3", "h2:0",
    "eh:2", "h2:1", "sh", "h3:0", "h2:3", "h3:1", "h2:2", "h2:4", "dn", "dx", "ed:0", "ed:1",
    "h3:3", "h3:2", "ed:3", "h3:4", "ed:2", "sd3", "sx", "sdn", "cb:0", "cb:1", "cb:3", "cb:2",
    "dx3", "sx3",
)


def dot(a, b):
    return jnp.dot(a, b, preferred_element_type=F32)


def kernel(
    tok_in,
    gain_in,
    gate_in,
    up_in,
    dn_in,
    shg_in,
    shu_in,
    shd_in,
    route,
    weight,
    gu,
    drow,
    shgu,
    sdrow,
    mixv,
    tok,
    gate_f,
    up_f,
    dn_f,
    shg_f,
    shu_f,
    shd_f,
    gain_col,
    scale_col,
    own,
    outgoing,
    arrived,
    gu_send,
    dn_send,
    dcol,
    sdcol,
    acc,
    hid,
    rsend,
    ret,
    comb,
    macc,
    ss,
    rs,
    ls,
):
    f = lax.axis_index("fs")
    c = lax.axis_index("tp")
    z, y = f // 4, f % 4
    x, k = c // 2, c % 2

    def fs_of(oz, oy):
        return ((z + oz) % 4) * 4 + (y + oy) % 4

    def tp_of(d, other=0):
        return ((x + d) % 4) * 2 + (k + other) % 2

    def fs_dev(oz, oy):
        return (fs_of(oz, oy), c)

    def tp_dev(d, other=0):
        return (f, tp_of(d, other))

    partner = tp_dev(0, 1)
    sent = []
    keys = {}

    def place(key):
        return keys.setdefault(key, len(keys))

    def send(src, dst, key, dev):
        copy = pltpu.make_async_remote_copy(
            src_ref=src,
            dst_ref=dst,
            send_sem=ss.at[len(sent)],
            recv_sem=rs.at[place(key)],
            device_id=dev,
            device_id_type=MESH,
        )
        copy.start()
        sent.append(copy)

    def arrive(dst, key):
        pltpu.make_async_remote_copy(
            src_ref=dst,
            dst_ref=dst,
            send_sem=ss.at[0],
            recv_sem=rs.at[place(key)],
            device_id=partner,
            device_id_type=MESH,
        ).wait_recv()

    def cols(tp_index, width):
        return pl.ds(pl.multiple_of(tp_index * width, width), width)

    def block(index, width):
        return pl.ds(pl.multiple_of(index * width, width), width)

    def load(n, src, dst):
        copy = pltpu.make_async_copy(src, dst, ls.at[n])
        copy.start()
        return copy

    quarter = TOK // 4
    tok_loads = [
        load(n, tok_in.at[pl.ds(n * quarter, quarter)], tok.at[pl.ds(n * quarter, quarter)])
        for n in range(4)
    ]
    shared_loads = [load(4, shg_in, shg_f), load(5, shu_in, shu_f), load(6, shd_in, shd_f)]

    barrier = pltpu.get_barrier_semaphore()
    for oz, oy in NEAR:
        pl.semaphore_signal(barrier, inc=1, device_id=fs_dev(oz, oy), device_id_type=MESH)
    for d in range(4):
        for other in range(2):
            if (d, other) != (0, 0):
                pl.semaphore_signal(
                    barrier, inc=1, device_id=tp_dev(d, other), device_id_type=MESH
                )

    def line(j, d):
        return fs_of(k * j + (1 - k) * d, (1 - k) * j + k * d)

    def spread_first(name, ref, height):
        piece = ref.at[block(f, height)]
        for d in (2, 1, 3):
            send(piece, piece, (name, 4 - d), (line(d, 0), c))

    def spread_second(name, ref, height):
        for j in (0, 1, 3, 2):
            piece = ref.at[block(line(j, 0), height)]
            if j:
                arrive(piece, (name, j))
            for d in (2, 1, 3):
                send(piece, piece, (name, j, 4 - d), (line(0, d), c))

    def spread_last(name, ref, height):
        for j in range(4):
            for d in (1, 2, 3):
                arrive(ref.at[block(line(j, d), height)], (name, j, d))

    r0, r1 = route[0:1, :], route[1:2, :]
    e_row = lax.broadcasted_iota(jnp.int32, (16, TOK), 0)
    is0, is1 = e_row == r0, e_row == r1
    named = jnp.where(is0 | is1, 1.0, 0.0).astype(BF16)
    before = jnp.where(
        lax.broadcasted_iota(jnp.int32, (TOK, TOK), 0)
        < lax.broadcasted_iota(jnp.int32, (TOK, TOK), 1),
        1.0,
        0.0,
    ).astype(BF16)
    earlier = dot(named, before)

    def target_of(r, hit):
        slot = jnp.sum(jnp.where(hit, earlier, 0.0), axis=0, keepdims=True)
        relative = (((r // 4) - z + 4) % 4) * 4 + ((r % 4) - y + 4) % 4
        return relative.astype(F32) * float(CAP) + slot

    t0, t1 = target_of(r0, is0), target_of(r1, is1)

    diag = lax.broadcasted_iota(jnp.int32, (256, 256), 0) == lax.broadcasted_iota(
        jnp.int32, (256, 256), 1
    )
    gain_col[...] = jnp.broadcast_to(
        jnp.sum(jnp.where(diag, gain_in[...], 0.0), axis=1, keepdims=True), (256, HB)
    )

    def square_step(i, carry):
        rows = pl.ds(pl.multiple_of(i * 16, 16), 16)
        total = jnp.zeros((16, HB), F32)
        for j in range(D // HB):
            v = tok[rows, j * HB : (j + 1) * HB].astype(F32)
            total = total + v * v
        scale_col[rows, :] = total
        return carry

    def own_step(i, carry):
        rows = pl.ds(pl.multiple_of(i * 64, 64), 64)
        s = lax.rsqrt(jnp.sum(scale_col[rows, :], axis=1, keepdims=True) * (1.0 / D) + norm_eps)
        scale_col[rows, :] = jnp.broadcast_to(s, (64, HB))
        own[rows, :] = (tok[rows, cols(c, COL)].astype(F32) * s).astype(BF16)
        return carry

    for n in range(4):
        tok_loads[n].wait()
        with jax.named_scope("square"):
            lax.fori_loop(n * 8, n * 8 + 8, square_step, 0, unroll=2)
    weight_loads = [load(7, gate_in, gate_f), load(8, up_in, up_f), load(9, dn_in, dn_f)]
    for copy in shared_loads:
        copy.wait()
    shgu[block(f, 256), 0:HB] = (shg_f[...] * gain_col[...]).astype(BF16)
    shgu[block(f, 256), HB : 2 * HB] = (shu_f[...] * gain_col[...]).astype(BF16)
    sdcol[block(f, 64), :] = shd_f[...].astype(BF16)
    with jax.named_scope("barrier"):
        pl.semaphore_wait(barrier, 22)
    spread_first("sh", shgu, 256)
    with jax.named_scope("own"):
        lax.fori_loop(0, TOK // 64, own_step, 0)

    def token_first(n):
        start, height = CHUNKS[n]
        for s in range(start // CAP, (start + height) // CAP):
            if s:
                arrive(arrived.at[pl.ds(s * CAP, CAP), cols(c, COL)], ("tok", s))
        piece = arrived.at[pl.ds(start, height), cols(c, COL)]
        send(piece, piece, ("xm", n), tp_dev(1))
        send(piece, piece, ("xp", n), tp_dev(3))
        send(piece, piece, ("kp", n, 0), partner)

    def token_second(n):
        start, height = CHUNKS[n]
        half = height // 2
        for name, d, then, on, skip in (("xm", 3, "ft", 1, 0), ("xp", 1, "fb", 3, half)):
            piece = arrived.at[pl.ds(start, height), cols(tp_of(d), COL)]
            arrive(piece, (name, n))
            part = arrived.at[pl.ds(start + skip, half), cols(tp_of(d), COL)]
            send(part, part, (then, n), tp_dev(on))
            send(piece, piece, ("kp", n, d), partner)

    def token_third(n):
        start, height = CHUNKS[n]
        half = height // 2
        for name, skip in (("ft", 0), ("fb", half)):
            part = arrived.at[pl.ds(start + skip, half), cols(tp_of(2), COL)]
            arrive(part, (name, n))
        piece = arrived.at[pl.ds(start, height), cols(tp_of(2), COL)]
        send(piece, piece, ("kp", n, 2), partner)

    def token_last(n):
        start, height = CHUNKS[n]
        for d in range(4):
            arrive(arrived.at[pl.ds(start, height), cols(tp_of(d, 1), COL)], ("kp", n, d))

    with jax.named_scope("dispatch"):
        for g in ORDER:
            s_row = (lax.broadcasted_iota(jnp.int32, (GROUP, TOK), 0) + g * GROUP).astype(F32)
            placing = jnp.where((s_row == t0) | (s_row == t1), 1.0, 0.0).astype(BF16)
            outgoing[g * GROUP : (g + 1) * GROUP, :] = dot(placing, own[...]).astype(BF16)
            for dy in ORDER:
                if (g, dy) != (0, 0):
                    there = ((4 - g) % 4) * 4 + (4 - dy) % 4
                    send(
                        outgoing.at[pl.ds((g * 4 + dy) * CAP, CAP)],
                        arrived.at[pl.ds(there * CAP, CAP), cols(c, COL)],
                        ("tok", there),
                        fs_dev(g, dy),
                    )
            if g == 0:
                arrived[0:CAP, cols(c, COL)] = outgoing[0:CAP, :]
    token_first(0)
    spread_first("sd", sdcol, 64)

    weight_loads[0].wait()
    weight_loads[1].wait()

    def gu_step(e, carry):
        gu_send[e, :, 0:HB] = (gate_f[e] * gain_col[...]).astype(BF16)
        gu_send[e, :, HB : 2 * HB] = (up_f[e] * gain_col[...]).astype(BF16)
        return carry

    with jax.named_scope("gu_cast"):
        lax.fori_loop(0, 16, gu_step, 0)
    for part in range(2):
        for oz, oy in FAR:
            there = ((4 - oz) % 4) * 4 + (4 - oy) % 4
            send(
                gu_send.at[fs_of(oz, oy), pl.ds(part * 128, 128)],
                gu.at[pl.ds(pl.multiple_of(f * 256 + part * 128, 128), 128)],
                ("gu", part, there),
                fs_dev(oz, oy),
            )
    gu[block(f, 256), :] = gu_send[f]
    with jax.named_scope("spread2_sh"):
        spread_second("sh", shgu, 256)
    weight_loads[2].wait()

    def dn_step(e, carry):
        dn_send[e] = dn_f[e].astype(BF16)
        return carry

    lax.fori_loop(0, 16, dn_step, 0)
    for oz, oy in FAR:
        there = ((4 - oz) % 4) * 4 + (4 - oy) % 4
        send(dn_send.at[fs_of(oz, oy)], dcol.at[block(f, 64)], ("dn", there), fs_dev(oz, oy))
    dcol[block(f, 64), :] = dn_send[f]

    def silu_times(gate, up):
        return (gate / (1.0 + jnp.exp(-gate)) * up).astype(BF16)

    def hidden_rows(g):
        return (g * GROUP, GROUP) if g < 4 else (ROWS, TOK)

    def hidden_first(g):
        start, height = hidden_rows(g)
        piece = hid.at[pl.ds(start, height), cols(c, HB)]
        send(piece, piece, ("hm", g), tp_dev(1))
        send(piece, piece, ("hp", g), tp_dev(3))
        send(piece, piece, ("hk", g, 0), partner)

    def hidden_second(g):
        start, height = hidden_rows(g)
        half = height // 2
        for name, d, then, on, skip in (("hm", 3, "ht", 1, 0), ("hp", 1, "hb", 3, half)):
            piece = hid.at[pl.ds(start, height), cols(tp_of(d), HB)]
            arrive(piece, (name, g))
            part = hid.at[pl.ds(start + skip, half), cols(tp_of(d), HB)]
            send(part, part, (then, g), tp_dev(on))
            send(piece, piece, ("hk", g, d), partner)

    def hidden_third(g):
        start, height = hidden_rows(g)
        half = height // 2
        for name, skip in (("ht", 0), ("hb", half)):
            part = hid.at[pl.ds(start + skip, half), cols(tp_of(2), HB)]
            arrive(part, (name, g))
        piece = hid.at[pl.ds(start, height), cols(tp_of(2), HB)]
        send(piece, piece, ("hk", g, 2), partner)

    def hidden_last(g):
        start, height = hidden_rows(g)
        for d in range(4):
            arrive(hid.at[pl.ds(start, height), cols(tp_of(d, 1), HB)], ("hk", g, d))

    def expert_hidden(g):
        for n in ((0, 1), (2,), (4,), (3,))[g]:
            token_last(n)
        rows = pl.ds(g * GROUP, GROUP)
        acc[0:GROUP] = jnp.zeros((GROUP, 2 * HB), F32)

        def step(i, carry):
            acc[0:GROUP] += dot(arrived[rows, block(i, COL)], gu[block(i, COL), :])
            return carry

        lax.fori_loop(0, 8, step, 0)
        hid[rows, cols(c, HB)] = silu_times(acc[0:GROUP, 0:HB], acc[0:GROUP, HB:])
        hidden_first(g)

    def expert_down(g):
        hidden_last(g)
        rows = pl.ds(g * GROUP, GROUP)
        rsend[rows, :] = dot(hid[rows, :], dcol[...]).astype(BF16)
        for dy in ORDER:
            if (g, dy) != (0, 0):
                there = ((4 - g) % 4) * 4 + (4 - dy) % 4
                send(
                    rsend.at[pl.ds((g * 4 + dy) * CAP, CAP)],
                    ret.at[pl.ds(there * CAP, CAP)],
                    ("ret", there),
                    fs_dev(g, dy),
                )
        if g == 0:
            ret[0:CAP, :] = rsend[0:CAP, :]

    def across(name, src, dst):
        for d in (2, 1, 3, 0):
            for other in range(2):
                if (d, other) != (0, 0):
                    send(
                        src.at[cols(tp_of(d, other), HB)],
                        dst.at[:, cols(c, COL)],
                        (name, (4 - d) % 4, other),
                        tp_dev(d, other),
                    )
        dst[:, cols(c, COL)] = src[cols(c, HB), :]

    def across_last(name, dst):
        for d in range(4):
            for other in range(2):
                if (d, other) != (0, 0):
                    arrive(dst.at[:, cols(tp_of(d, other), COL)], (name, d, other))

    def norm_step(i, carry):
        rows = pl.ds(pl.multiple_of(i * 16, 16), 16)
        tok[rows, :] = (tok[rows, :].astype(F32) * scale_col[rows, 0:1]).astype(BF16)
        return carry

    def combine_weights():
        packed = jnp.concatenate([t0, t1, weight[...], jnp.zeros((4, TOK), F32)], axis=0)
        by_token = packed.T
        for g in range(4):
            s_col = (lax.broadcasted_iota(jnp.int32, (TOK, GROUP), 1) + g * GROUP).astype(F32)
            comb[:, g * GROUP : (g + 1) * GROUP] = (
                jnp.where(s_col == by_token[:, 0:1], by_token[:, 2:3], 0.0)
                + jnp.where(s_col == by_token[:, 1:2], by_token[:, 3:4], 0.0)
            ).astype(BF16)

    def gu_last():
        for part in range(2):
            for oz, oy in NEAR:
                start = pl.multiple_of(fs_of(oz, oy) * 256 + part * 128, 128)
                arrive(gu.at[pl.ds(start, 128)], ("gu", part, oz * 4 + oy))

    def dn_last():
        for oz, oy in NEAR:
            arrive(dcol.at[block(fs_of(oz, oy), 64)], ("dn", oz * 4 + oy))

    def shared_hidden():
        spread_last("sh", shgu, 256)
        acc[...] = jnp.zeros((TOK, 2 * HB), F32)

        def step(i, carry):
            acc[...] += dot(tok[:, block(i, COL)], shgu[block(i, COL), :])
            return carry

        lax.fori_loop(0, 8, step, 0)
        hid[ROWS : ROWS + TOK, cols(c, HB)] = silu_times(acc[:, 0:HB], acc[:, HB:])
        hidden_first(4)

    def shared_down():
        hidden_last(4)
        macc[...] = dot(hid[ROWS : ROWS + TOK, :], sdcol[...])

    def combine(g):
        oz = (4 - g) % 4
        for oy in ORDER:
            if (oz, oy) != (0, 0):
                s = oz * 4 + oy
                arrive(ret.at[pl.ds(s * CAP, CAP)], ("ret", s))
        macc[...] += dot(comb[:, oz * GROUP : (oz + 1) * GROUP], ret[oz * GROUP : (oz + 1) * GROUP])

    steps = dict(
        t1=token_first,
        t2=token_second,
        t3=token_third,
        eh=expert_hidden,
        h2=hidden_second,
        h3=hidden_third,
        ed=expert_down,
        cb=combine,
    )
    singles = dict(
        norm=lambda: lax.fori_loop(0, TOK // 16, norm_step, 0, unroll=2),
        comb=combine_weights,
        gu=gu_last,
        dn=dn_last,
        sd2=lambda: spread_second("sd", sdcol, 64),
        sd3=lambda: spread_last("sd", sdcol, 64),
        sh=shared_hidden,
        sdn=shared_down,
        dx=lambda: across("dx", dcol, drow),
        sx=lambda: across("sx", sdcol, sdrow),
        dx3=lambda: across_last("dx", drow),
        sx3=lambda: across_last("sx", sdrow),
    )
    for word in PLAN:
        with jax.named_scope(word.replace(":", "_")):
            if ":" in word:
                name, n = word.split(":")
                steps[name](int(n))
            else:
                singles[word]()
    mixv[...] = macc[...].astype(BF16)
    with jax.named_scope("drain"):
        for copy in sent:
            copy.wait_send()


def writer(gu, drow, shgu, sdrow, mixv, eg, eu, ed, sg, su, sd, mix, sems):
    copies = [
        pltpu.make_async_copy(src, dst, sems.at[n])
        for n, (src, dst) in enumerate(
            (
                (gu.at[:, pl.ds(0, HB)], eg.at[0]),
                (gu.at[:, pl.ds(HB, HB)], eu.at[0]),
                (drow, ed.at[0]),
                (shgu.at[:, pl.ds(0, HB)], sg),
                (shgu.at[:, pl.ds(HB, HB)], su),
                (sdrow, sd),
                (mixv, mix),
            )
        )
    ]
    for copy in copies:
        copy.start()
    for copy in copies:
        copy.wait()


def on_device(
    tokens,
    norm_gain,
    gate_train,
    up_train,
    down_train,
    shared_gate_train,
    shared_up_train,
    shared_down_train,
    route_expert,
    route_weight,
):
    hbm = pl.BlockSpec(memory_space=pl.ANY)
    vmem = pl.BlockSpec(memory_space=pltpu.VMEM)
    kept = pl.pallas_call(
        kernel,
        out_shape=(
            pltpu.VMEM((D, 2 * HB), BF16),
            pltpu.VMEM((HB, D), BF16),
            pltpu.VMEM((D, 2 * HB), BF16),
            pltpu.VMEM((HB, D), BF16),
            pltpu.VMEM((TOK, COL), BF16),
        ),
        in_specs=[hbm, vmem, hbm, hbm, hbm, hbm, hbm, hbm, vmem, vmem],
        out_specs=(vmem,) * 5,
        scratch_shapes=[
            pltpu.VMEM((TOK, D), BF16),
            pltpu.VMEM((16, 256, HB), F32),
            pltpu.VMEM((16, 256, HB), F32),
            pltpu.VMEM((16, 64, COL), F32),
            pltpu.VMEM((256, HB), F32),
            pltpu.VMEM((256, HB), F32),
            pltpu.VMEM((64, COL), F32),
            pltpu.VMEM((256, HB), F32),
            pltpu.VMEM((TOK, HB), F32),
            pltpu.VMEM((TOK, COL), BF16),
            pltpu.VMEM((ROWS, COL), BF16),
            pltpu.VMEM((ROWS, D), BF16),
            pltpu.VMEM((16, 256, 2 * HB), BF16),
            pltpu.VMEM((16, 64, COL), BF16),
            pltpu.VMEM((H, COL), BF16),
            pltpu.VMEM((H, COL), BF16),
            pltpu.VMEM((TOK, 2 * HB), F32),
            pltpu.VMEM((ROWS + TOK, H), BF16),
            pltpu.VMEM((ROWS, COL), BF16),
            pltpu.VMEM((ROWS, COL), BF16),
            pltpu.VMEM((TOK, ROWS), BF16),
            pltpu.VMEM((TOK, COL), F32),
            pltpu.SemaphoreType.DMA((224,)),
            pltpu.SemaphoreType.DMA((224,)),
            pltpu.SemaphoreType.DMA((10,)),
        ],
        compiler_params=pltpu.CompilerParams(
            collective_id=0, has_side_effects=True, vmem_limit_bytes=54 * 1024 * 1024
        ),
        name="layer",
    )(
        tokens,
        norm_gain.reshape(1, 256),
        gate_train,
        up_train,
        down_train,
        shared_gate_train,
        shared_up_train,
        shared_down_train,
        route_expert.T,
        route_weight.T,
    )
    return pl.pallas_call(
        writer,
        out_shape=(
            jax.ShapeDtypeStruct((1, D, HB), BF16),
            jax.ShapeDtypeStruct((1, D, HB), BF16),
            jax.ShapeDtypeStruct((1, HB, D), BF16),
            jax.ShapeDtypeStruct((D, HB), BF16),
            jax.ShapeDtypeStruct((D, HB), BF16),
            jax.ShapeDtypeStruct((HB, D), BF16),
            jax.ShapeDtypeStruct((TOK, COL), BF16),
        ),
        in_specs=[vmem] * 5,
        out_specs=(hbm,) * 7,
        scratch_shapes=[pltpu.SemaphoreType.DMA((7,))],
        compiler_params=pltpu.CompilerParams(vmem_limit_bytes=1024 * 1024),
        name="writer",
    )(*(pltpu.with_memory_space_constraint(a, pltpu.VMEM) for a in kept))


def solution(mesh):
    placed = (
        P("fs", None),
        P("fs"),
        P(None, "fs", "tp"),
        P(None, "fs", "tp"),
        P(None, "fs", "tp"),
        P("fs", "tp"),
        P("fs", "tp"),
        P("fs", "tp"),
        P("fs", None),
        P("fs", None),
    )
    return jax.shard_map(
        on_device,
        mesh=mesh,
        in_specs=placed,
        out_specs=(
            P("fs", None, "tp"),
            P("fs", None, "tp"),
            P("fs", "tp", None),
            P(None, "tp"),
            P(None, "tp"),
            P("tp", None),
            P("fs", "tp"),
        ),
        check_vma=False,
    )
```

time: 145 us -> 122 us (0.84)
  Pallas kernels: 135 us -> 120 us
  local copies, waits for them, and re-layouts: 8.07 us -> 0 us
    pallas_call x1 -> x2, Pallas kernels: 135 us -> 120 us  [the longest x1 117 us: on_device(): pl.pallas_call(kernel, out_shape=(pltpu.VMEM((D, 2 * HB), BF16), pltpu.VM...]
    unnamed x19 -> x0, local copies, waits for them, and re-layouts: 8.07 us -> none
where the time goes in v2:
time: 122 us; the launch traced here: 121 us
  Pallas kernels  120 us (98%)
    pallas_call x1, Pallas kernels, on_device(): pl.pallas_call(kernel, out_shape=(pltpu.VMEM((D, 2 * HB), BF16), pltpu.VM...  117 us
    pallas_call x1, Pallas kernels, on_device(): pl.pallas_call(writer, out_shape=(jax.ShapeDtypeStruct((1, D, HB), BF16),...  2.87 us

profile of v2, /device:TPU:1, one launch (start us, length us, event | category | flops | bytes accessed | tf_op | source)
XLA Modules:
  0.0 120.5 jit_solution(2770479902900481311)
XLA Ops:
  0.6 117.0 %layer.1 = (bf16[4096,256]{1,0:T(8,128)(2,1)S(1)}, bf16[128,4096]{1,0:T(8,128)(2,1)S(1)}, bf16[4096,256]{1,0:T(8,128)(2,1)S(1)}, bf16[128,4096]{1,0:T(8,128)(2,1)S(1)}, bf16[512,512]{1,0:T(8,128)(2,1)S(1)}) custom-call(bf16[512,4096]{1,0:T(8,128)(2,1)} %tok_in.1, f32[1,256]{1,0:T(1,128)} %bitcast.5, f32[16,256,128]{2,1,0:T(8,128)} %gate_in.1, ...), custom_call_target="tpu_custom_call" | custom-call | tf_op jit(solution)/shard_map/layer/pallas_call | solution.py:527
  117.6 2.9 %writer.1 = (bf16[1,4096,128]{2,1,0:T(8,128)(2,1)}, bf16[1,4096,128]{2,1,0:T(8,128)(2,1)}, bf16[1,128,4096]{2,1,0:T(8,128)(2,1)}, bf16[4096,128]{1,0:T(8,128)(2,...) custom-call(bf16[4096,256]{1,0:T(8,128)(2,1)S(1)} %get-tuple-element.12.gu, ...), custom_call_target="tpu_custom_call" | custom-call | tf_op jit(solution)/shard_map/writer/pallas_call | solution.py:581

commit v3 on v2

--- a/solution.py
+++ b/solution.py
@@ -24,11 +24,11 @@
 CHUNKS = ((0, CAP), (CAP, 3 * CAP), (GROUP, GROUP), (3 * GROUP, GROUP), (2 * GROUP, GROUP))
 
 PLAN = (
-    "t1:1", "t2:0", "t1:2", "t2:1", "t3:0", "sd2", "t1:3", "t2:2", "t3:1", "comb", "norm",
-    "t1:4", "t2:3", "t3:2", "t2:4", "t3:3", "gu", "eh:0", "eh:1", "t3:4", "eh:3", "h2:0",
-    "eh:2", "h2:1", "sh", "h3:0", "h2:3", "h3:1", "h2:2", "h2:4", "dn", "dx", "ed:0", "ed:1",
-    "h3:3", "h3:2", "ed:3", "h3:4", "ed:2", "sd3", "sx", "sdn", "cb:0", "cb:1", "cb:3", "cb:2",
-    "dx3", "sx3",
+    "t1:0", "sd1", "gu1", "gu2", "sh2", "dn1", "t1:1", "t2:0", "comb", "norm", "t1:2", "t2:1",
+    "t3:0", "t1:3", "t1:4", "t2:2", "t3:1", "t2:3", "t3:2", "sd2", "t2:4", "t3:3", "gu", "eh:0",
+    "eh:1", "t3:4", "eh:3", "h2:0", "eh:2", "h2:1", "sh", "h3:0", "h2:3", "h3:1", "h2:2",
+    "h2:4", "dn", "dxa", "dxb", "ed:0", "ed:1", "h3:3", "h3:2", "ed:3", "h3:4", "ed:2", "sd3",
+    "sxa", "sxb", "sdn", "cb:0", "cb:1", "cb:3", "cb:2", "dx3", "sx3",
 )
 
 
@@ -281,20 +281,19 @@
                     )
             if g == 0:
                 arrived[0:CAP, cols(c, COL)] = outgoing[0:CAP, :]
-    token_first(0)
-    spread_first("sd", sdcol, 64)
-
-    weight_loads[0].wait()
-    weight_loads[1].wait()
-
     def gu_step(e, carry):
         gu_send[e, :, 0:HB] = (gate_f[e] * gain_col[...]).astype(BF16)
         gu_send[e, :, HB : 2 * HB] = (up_f[e] * gain_col[...]).astype(BF16)
         return carry
 
-    with jax.named_scope("gu_cast"):
+    def gu_first():
+        weight_loads[0].wait()
+        weight_loads[1].wait()
         lax.fori_loop(0, 16, gu_step, 0)
-    for part in range(2):
+        gu[block(f, 256), :] = gu_send[f]
+        gu_part(0)
+
+    def gu_part(part):
         for oz, oy in FAR:
             there = ((4 - oz) % 4) * 4 + (4 - oy) % 4
             send(
@@ -303,20 +302,18 @@
                 ("gu", part, there),
                 fs_dev(oz, oy),
             )
-    gu[block(f, 256), :] = gu_send[f]
-    with jax.named_scope("spread2_sh"):
-        spread_second("sh", shgu, 256)
-    weight_loads[2].wait()
 
     def dn_step(e, carry):
         dn_send[e] = dn_f[e].astype(BF16)
         return carry
 
-    lax.fori_loop(0, 16, dn_step, 0)
-    for oz, oy in FAR:
-        there = ((4 - oz) % 4) * 4 + (4 - oy) % 4
-        send(dn_send.at[fs_of(oz, oy)], dcol.at[block(f, 64)], ("dn", there), fs_dev(oz, oy))
-    dcol[block(f, 64), :] = dn_send[f]
+    def dn_first():
+        weight_loads[2].wait()
+        lax.fori_loop(0, 16, dn_step, 0)
+        for oz, oy in FAR:
+            there = ((4 - oz) % 4) * 4 + (4 - oy) % 4
+            send(dn_send.at[fs_of(oz, oy)], dcol.at[block(f, 64)], ("dn", there), fs_dev(oz, oy))
+        dcol[block(f, 64), :] = dn_send[f]
 
     def silu_times(gate, up):
         return (gate / (1.0 + jnp.exp(-gate)) * up).astype(BF16)
@@ -359,14 +356,8 @@
         for n in ((0, 1), (2,), (4,), (3,))[g]:
             token_last(n)
         rows = pl.ds(g * GROUP, GROUP)
-        acc[0:GROUP] = jnp.zeros((GROUP, 2 * HB), F32)
-
-        def step(i, carry):
-            acc[0:GROUP] += dot(arrived[rows, block(i, COL)], gu[block(i, COL), :])
-            return carry
-
-        lax.fori_loop(0, 8, step, 0)
-        hid[rows, cols(c, HB)] = silu_times(acc[0:GROUP, 0:HB], acc[0:GROUP, HB:])
+        both = dot(arrived[rows, :], gu[...])
+        hid[rows, cols(c, HB)] = silu_times(both[:, 0:HB], both[:, HB:])
         hidden_first(g)
 
     def expert_down(g):
@@ -385,8 +376,8 @@
         if g == 0:
             ret[0:CAP, :] = rsend[0:CAP, :]
 
-    def across(name, src, dst):
-        for d in (2, 1, 3, 0):
+    def across(name, src, dst, some):
+        for d in some:
             for other in range(2):
                 if (d, other) != (0, 0):
                     send(
@@ -395,7 +386,8 @@
                         (name, (4 - d) % 4, other),
                         tp_dev(d, other),
                     )
-        dst[:, cols(c, COL)] = src[cols(c, HB), :]
+        if 0 in some:
+            dst[:, cols(c, COL)] = src[cols(c, HB), :]
 
     def across_last(name, dst):
         for d in range(4):
@@ -467,12 +459,20 @@
         comb=combine_weights,
         gu=gu_last,
         dn=dn_last,
+        gu1=gu_first,
+        gu2=lambda: gu_part(1),
+        dn1=dn_first,
+        sh1=lambda: spread_first("sh", shgu, 256),
+        sh2=lambda: spread_second("sh", shgu, 256),
+        sd1=lambda: spread_first("sd", sdcol, 64),
         sd2=lambda: spread_second("sd", sdcol, 64),
         sd3=lambda: spread_last("sd", sdcol, 64),
         sh=shared_hidden,
         sdn=shared_down,
-        dx=lambda: across("dx", dcol, drow),
-        sx=lambda: across("sx", sdcol, sdrow),
+        dxa=lambda: across("dx", dcol, drow, (2, 0)),
+        dxb=lambda: across("dx", dcol, drow, (1, 3)),
+        sxa=lambda: across("sx", sdcol, sdrow, (2, 0)),
+        sxb=lambda: across("sx", sdcol, sdrow, (1, 3)),
         dx3=lambda: across_last("dx", drow),
         sx3=lambda: across_last("sx", sdrow),
     )

time: 122 us -> 119 us (0.975)
  Pallas kernels: 120 us -> 118 us
    pallas_call x1, Pallas kernels: 117 us -> 115 us  [on_device(): pl.pallas_call(kernel, out_shape=(pltpu.VMEM((D, 2 * HB), BF16), pltpu.VM...]
where the time goes in v3:
time: 119 us; the launch traced here: 118 us
  Pallas kernels  118 us (99%)
    pallas_call x1, Pallas kernels, on_device(): pl.pallas_call(kernel, out_shape=(pltpu.VMEM((D, 2 * HB), BF16), pltpu.VM...  115 us
    pallas_call x1, Pallas kernels, on_device(): pl.pallas_call(writer, out_shape=(jax.ShapeDtypeStruct((1, D, HB), BF16),...  2.87 us

profile of v3, /device:TPU:1, one launch (start us, length us, event | category | flops | bytes accessed | tf_op | source)
XLA Modules:
  0.0 118.5 jit_solution(12939819102144254082)
XLA Ops:
  0.6 115.0 %layer.1 = (bf16[4096,256]{1,0:T(8,128)(2,1)S(1)}, bf16[128,4096]{1,0:T(8,128)(2,1)S(1)}, bf16[4096,256]{1,0:T(8,128)(2,1)S(1)}, bf16[128,4096]{1,0:T(8,128)(2,1)S(1)}, bf16[512,512]{1,0:T(8,128)(2,1)S(1)}) custom-call(bf16[512,4096]{1,0:T(8,128)(2,1)} %tok_in.1, f32[1,256]{1,0:T(1,128)} %bitcast.5, f32[16,256,128]{2,1,0:T(8,128)} %gate_in.1, ...), custom_call_target="tpu_custom_call" | custom-call | tf_op jit(solution)/shard_map/layer/pallas_call | solution.py:527
  115.6 2.9 %writer.1 = (bf16[1,4096,128]{2,1,0:T(8,128)(2,1)}, bf16[1,4096,128]{2,1,0:T(8,128)(2,1)}, bf16[1,128,4096]{2,1,0:T(8,128)(2,1)}, bf16[4096,128]{1,0:T(8,128)(2,...) custom-call(bf16[4096,256]{1,0:T(8,128)(2,1)S(1)} %get-tuple-element.12.gu, ...), custom_call_target="tpu_custom_call" | custom-call | tf_op jit(solution)/shard_map/writer/pallas_call | solution.py:581

commit v4 on v3

--- a/solution.py
+++ b/solution.py
@@ -218,7 +218,7 @@
     for n in range(4):
         tok_loads[n].wait()
         with jax.named_scope("square"):
-            lax.fori_loop(n * 8, n * 8 + 8, square_step, 0, unroll=2)
+            lax.fori_loop(n * 8, n * 8 + 8, square_step, 0, unroll=4)
     weight_loads = [load(7, gate_in, gate_f), load(8, up_in, up_f), load(9, dn_in, dn_f)]
     for copy in shared_loads:
         copy.wait()
@@ -229,7 +229,7 @@
         pl.semaphore_wait(barrier, 22)
     spread_first("sh", shgu, 256)
     with jax.named_scope("own"):
-        lax.fori_loop(0, TOK // 64, own_step, 0)
+        lax.fori_loop(0, TOK // 64, own_step, 0, unroll=4)
 
     def token_first(n):
         start, height = CHUNKS[n]

time: 119 us -> 119 us (level)
  no operation moved by 1% of the time
where the time goes in v4:
time: 119 us
  Pallas kernels  119 us (100%)
    pallas_call x1, Pallas kernels, on_device(): pl.pallas_call(kernel, out_shape=(pltpu.VMEM((D, 2 * HB), BF16), pltpu.VM...  116 us
    pallas_call x1, Pallas kernels, on_device(): pl.pallas_call(writer, out_shape=(jax.ShapeDtypeStruct((1, D, HB), BF16),...  2.87 us

profile of v4, /device:TPU:1, one launch (start us, length us, event | category | flops | bytes accessed | tf_op | source)
XLA Modules:
  0.0 119.2 jit_solution(12503338749103253304)
XLA Ops:
  0.6 115.7 %layer.1 = (bf16[4096,256]{1,0:T(8,128)(2,1)S(1)}, bf16[128,4096]{1,0:T(8,128)(2,1)S(1)}, bf16[4096,256]{1,0:T(8,128)(2,1)S(1)}, bf16[128,4096]{1,0:T(8,128)(2,1)S(1)}, bf16[512,512]{1,0:T(8,128)(2,1)S(1)}) custom-call(bf16[512,4096]{1,0:T(8,128)(2,1)} %tok_in.1, f32[1,256]{1,0:T(1,128)} %bitcast.5, f32[16,256,128]{2,1,0:T(8,128)} %gate_in.1, ...), custom_call_target="tpu_custom_call" | custom-call | tf_op jit(solution)/shard_map/layer/pallas_call | solution.py:527
  116.3 2.9 %writer.1 = (bf16[1,4096,128]{2,1,0:T(8,128)(2,1)}, bf16[1,4096,128]{2,1,0:T(8,128)(2,1)}, bf16[1,128,4096]{2,1,0:T(8,128)(2,1)}, bf16[4096,128]{1,0:T(8,128)(2,...) custom-call(bf16[4096,256]{1,0:T(8,128)(2,1)S(1)} %get-tuple-element.12.gu, ...), custom_call_target="tpu_custom_call" | custom-call | tf_op jit(solution)/shard_map/writer/pallas_call | solution.py:581
